TPU v7x, 32 devices: a whole 2x2x4 slice. The times are simulated.
32 devices in a mesh: gr: 2 (over y), sp: 4 (over z), tp: 4 (over x, core).
Axes of the slice: x: 2, y: 2, z: 4, core: 2. Of those that a mesh axis runs over, the one named last changes fastest.
Arguments:
- tokens: bfloat16 [8, 768, 4096], P('gr', 'sp'), parts along dimension 0, may hold values from -50 to 50
- new_tokens: bfloat16 [8, 4096], P('gr'), parts along dimension 0, may hold values from -6 to 6
- in_gain: float32 [4096], replicated, may hold values from 0.1 to 1.9
- w_forget: bfloat16 [4096, 2048], P(None, 'tp'), may hold values from -0.09375 to 0.09375
- w_value: bfloat16 [4096, 2048], P(None, 'tp'), may hold values from -0.75 to 0.75
- gap: float32 [16, 128], P('tp'), may hold values from 0 to 0.06
- decay_shift: float32 [8, 768, 16], P('gr', 'sp', 'tp'), parts along dimension 0, may hold values from -3 to 0
- query: bfloat16 [8, 16, 128], P('gr', 'tp', 'sp'), parts along dimension 0, may hold values from -6 to 6
- out_gain: float32 [16, 128], P('tp'), may hold values from 0.1 to 1.9
Outputs:
- cache: bfloat16 [8, 16, 128, 128], P('gr', 'tp', 'sp'), parts along dimension 0
- read: float32 [8, 16, 128], P('gr', 'tp'), parts along dimension 0
There are 2 independent parts, one for each index of `gr`. A program takes and returns all parts, laid end to end along the dimension named above; an argument that names none is the same for every part. Nothing has to cross between parts.
All inputs are finite; a program needn't handle non-finite values.
Results may differ from a plain program's by a relative error of at most 0.0065.
Values sent between devices are 32-bit elements; how exact they have to be, the bound alone decides.
A program may use at most 64 MiB of HBM per device.

v0:
```python
import jax
import jax.numpy as jnp
from jax import lax
from jax.sharding import PartitionSpec as P

epsilon = 1e-06


def normalize(row_block, gain_row):
    widened = row_block.astype(jnp.float32)
    scaled = widened * lax.rsqrt(jnp.mean(widened * widened, axis=-1, keepdims=True) + epsilon)
    return (scaled * gain_row).astype(jnp.bfloat16)


def settle(received):
    stacked, block_sums = received
    later_sum = jnp.cumsum(block_sums[::-1], axis=0)[::-1] - block_sums
    return jnp.sum(jnp.exp(later_sum)[..., None] * stacked, axis=0)


def local(tokens, new_tokens, in_gain, w_forget, w_value, gap, decay_shift, query, out_gain):
    seq_count, seg_len, model_width = tokens.shape
    head_count, key_dim = gap.shape
    val_dim = out_gain.shape[1]
    row_count = key_dim // lax.axis_size("sp")
    unit_norm_rows = normalize(tokens.reshape(seq_count * seg_len, model_width), in_gain)
    forget_pre = jnp.dot(unit_norm_rows, w_forget, preferred_element_type=jnp.float32).reshape(
        seq_count, seg_len, head_count, key_dim
    )
    values = jnp.dot(unit_norm_rows, w_value, preferred_element_type=jnp.float32).astype(
        jnp.bfloat16
    )
    values = values.reshape(seq_count, seg_len, head_count, val_dim)
    key_gate = gap * jax.nn.sigmoid(-forget_pre)
    forget_logarithm = jnp.log1p(-key_gate) + decay_shift[:, :, :, None]
    totals = jnp.sum(forget_logarithm, axis=1)
    within = totals[:, None] - jnp.cumsum(forget_logarithm, axis=1)
    weights = (key_gate * jnp.exp(within)).astype(jnp.bfloat16)
    pieces = jnp.einsum("sthi,sthj->shij", weights, values, preferred_element_type=jnp.float32)
    full_state = settle(
        (
            lax.all_to_all(pieces[None], "sp", split_axis=3, concat_axis=0, tiled=True),
            lax.all_to_all(totals[None], "sp", split_axis=3, concat_axis=0, tiled=True),
        )
    )
    cache = full_state.astype(jnp.bfloat16)
    row_start = lax.axis_index("sp") * row_count
    normed_new = normalize(new_tokens, in_gain)
    new_pre = jnp.dot(normed_new, w_forget, preferred_element_type=jnp.float32).reshape(
        seq_count, head_count, key_dim
    )
    new_key = lax.dynamic_slice_in_dim(gap * jax.nn.sigmoid(-new_pre), row_start, row_count, 2)
    new_values = lax.optimization_barrier(
        jnp.dot(normed_new, w_value, preferred_element_type=jnp.float32).astype(jnp.bfloat16)
    )
    new_values = new_values.astype(jnp.float32).reshape(seq_count, head_count, val_dim)
    updated = (1.0 - new_key)[..., None] * full_state + new_key[..., None] * new_values[
        :, :, None, :
    ]
    partial_value = jnp.einsum(
        "shi,shij->shj", query.astype(jnp.float32), updated, precision=lax.Precision.HIGHEST
    )
    read_raw = lax.psum(partial_value, "sp")
    read = (
        read_raw
        * lax.rsqrt(jnp.mean(read_raw * read_raw, axis=-1, keepdims=True) + epsilon)
        * out_gain
    )
    return (cache, read)


def solution(mesh):
    return jax.shard_map(
        local,
        mesh=mesh,
        in_specs=(
            P("gr", "sp", None),
            P("gr", None),
            P(),
            P(None, "tp"),
            P(None, "tp"),
            P("tp", None),
            P("gr", "sp", "tp"),
            P("gr", "tp", "sp"),
            P("tp", None),
        ),
        out_specs=(P("gr", "tp", "sp", None), P("gr", "tp", None)),
        check_vma=False,
    )
```

profile of v0, /device:TPU:0, one launch (start us, length us, event | category | flops | bytes accessed | tf_op | source)
XLA Modules:
  0.0 92.6 jit_solution(18022183195930927783)
XLA Ops:
  0.7 6.4 %copy.34 = bf16[512,4096]{1,0:T(8,128)(2,1)} copy(bf16[512,4096]{0,1:T(8,128)(2,1)} %bitcast.65) | data formatting | bytes 8388608 | tf_op jit(solution)/shard_map/dot_general | solution.py:27
  7.1 4.2 %multiply_reduce_fusion = f32[4,192]{1,0:T(4,128)S(1)} fusion(bf16[4,192,4096]{2,1,0:T(8,128)(2,1)} %param.9), kind=kLoop, calls=%fused_computation.4 | loop fusion | flops 9436416 | bytes 6294528 | tf_op jit(solution)/shard_map/reduce_sum | solution.py:11
  11.7 6.4 %fusion.15 = (f32[4,128,4,192]{1,3,2,0:T(8,128)S(1)}, f32[4,192,4,128]{3,1,2,0:T(8,128)S(1)}) fusion(f32[4,4,192]{2,1,0:T(4,128)S(1)} %bitcast.79, f32[128,4]{0,1:T(4,128)S(1)} %bitcast.78, bf16[4,128,4096,1]{2,1,0,3:T(8,128)(2,1)} %bitcast.70, f32[4096]{0:T(1024)S(1)} %copy-done.6, f32[4,192]{1,0:T(4,128)S(1)} %add_rsqrt_fusion, ...), kind=kOutput, calls=%fused_computation.19 | convolution fusion | flops 3235774464 | bytes 13665280 | tf_op jit(solution)/shard_map/dot_general | solution.py:27
  18.1 1.1 %copy-done.4 = f32[4,192,4,128]{3,1,2,0:T(8,128)} copy-done((f32[4,192,4,128]{3,1,2,0:T(8,128)}, f32[4,192,4,128]{3,1,2,0:T(8,128)S(1)}, u32[]{:S(2)}) %copy-start.4) | copy-done | bytes 1572888
  19.3 0.7 add_reduce_fusion
  20.2 0.9 reshape.91
  21.0 6.3 %all-to-all-start = ((f32[4,1,512]{2,1,0:T(1,128)}), f32[4,1,512]{2,1,0:T(1,128)S(1)}, u32[]{:S(2)}, u32[]{:S(2)}) async-start(f32[4,1,512]{2,1,0:T(1,128)} %reshape.91), calls=%async_computation | async-start | bytes 16384 | tf_op jit(solution)/shard_map/all_to_all | solution.py:43
  27.7 1.6 %fusion.8 = f32[4,128,4,2,128]{1,3,2,4,0:T(2,128)S(1)} fusion(f32[4,128,4,2,128]{1,4,3,2,0:T(8,128)S(1)} %bitcast.68), kind=kOutput, calls=%fused_computation.10 | output fusion | flops 66584576 | bytes 4194304 | tf_op jit(solution)/shard_map/reduce-window
  29.3 1.3 %copy-done.2 = f32[4,128,4,2,128]{1,3,2,4,0:T(2,128)} copy-done((f32[4,128,4,2,128]{1,3,2,4,0:T(2,128)}, f32[4,128,4,2,128]{1,3,2,4,0:T(2,128)S(1)}, u32[]{:S(2)}) %copy-start.2) | copy-done | bytes 2097176
  30.8 1.9 %broadcast_add_fusion = f32[4,128,1,8,128]{1,3,2,4,0:T(8,128)S(1)} fusion(f32[4,128,1,8,128]{1,3,2,4,0:T(8,128)} %bitcast.66, f32[4,128,1,8]{1,3,2,0:T(8,128)S(1)} %bitcast.76), kind=kLoop, calls=%fused_computation.29 | loop fusion | flops 524288 | bytes 4210688 | tf_op jit(solution)/shard_map/reduce_window_sum
  32.6 1.7 %copy.24 = f32[4,128,4,2,128]{1,4,3,2,0:T(8,128)} copy(f32[4,128,4,2,128]{1,3,2,4,0:T(2,128)S(1)} %bitcast.67) | data formatting | bytes 4194304 | tf_op jit(solution)/shard_map/reduce_window_sum
  34.4 2.7 %fusion.1 = bf16[768,4096]{1,0:T(8,128)(2,1)S(1)} fusion(f32[4096]{0:T(1024)S(1)} %copy-done.6, f32[768]{0:T(1024)S(1)} %rsqrt.29, bf16[4,192,4096]{2,1,0:T(8,128)(2,1)S(1)} %bitcast.64), kind=kLoop, calls=%fused_computation.2 | loop fusion | flops 12582912 | bytes 12602368 | tf_op jit(solution)/shard_map/convert_element_type | solution.py:12
  37.1 6.6 %convolution_convert_fusion = bf16[768,512]{1,0:T(8,128)(2,1)} fusion(bf16[768,4096]{1,0:T(8,128)(2,1)S(1)} %fusion.1, bf16[4096,512]{1,0:T(8,128)(2,1)} %param.13), kind=kOutput, calls=%fused_computation.22 | convolution fusion | flops 3221618688 | bytes 11272192 | tf_op jit(solution)/shard_map/dot_general | solution.py:30
  43.8 1.7 %reshape.84 = bf16[4,192,4,128]{3,2,1,0:T(4,128)(2,1)S(1)} reshape(bf16[768,512]{1,0:T(8,128)(2,1)} %convolution_convert_fusion) | data formatting | bytes 1572864 | tf_op jit(solution)/shard_map/reshape | solution.py:33
  45.5 2.1 %convolution_bitcast_fusion = f32[1,4,4,128,128]{4,3,2,1,0:T(8,128)S(1)} fusion(f32[4,256,4,128]{3,1,2,0:T(8,128)S(1)} %bitcast.69, f32[4,192,4,128]{3,1,2,0:T(8,128)} %copy-done.4, bf16[4,192,4,128]{3,2,1,0:T(4,128)(2,1)S(1)} %reshape.84, f32[4,4,128]{2,1,0:T(4,128)S(1)} %add_reduce_fusion, f32[4,128]{1,0:T(4,128)S(1)} %copy-done.7), kind=kOutput, calls=%fused_computation.23 | convolution fusion | flops 102236160 | bytes 4990976 | tf_op jit(solution)/shard_map/sthi,sthj->shij/dot_general | solution.py:39
  47.8 1.7 %copy.26 = f32[1,4,4,128,128]{4,2,1,0,3:T(4,128)} copy(f32[1,4,4,128,128]{4,3,2,1,0:T(8,128)S(1)} %convolution_bitcast_fusion) | data formatting | bytes 2097152 | tf_op jit(solution)/shard_map/broadcast_in_dim | solution.py:42
  49.5 5.1 %all-to-all-start.1 = ((f32[1,4,4,128,128]{4,2,1,0,3:T(4,128)}), f32[1,4,4,128,128]{4,2,1,0,3:T(4,128)S(1)}, u32[]{:S(2)}, u32[]{:S(2)}) async-start(f32[1,4,4,128,128]{4,2,1,0,3:T(4,128)} %copy.26), calls=%async_computation.1 | async-start | bytes 2097152 | tf_op jit(solution)/shard_map/all_to_all | solution.py:42
  54.6 2.9 %convolution_convert_fusion.1 = bf16[4,512]{1,0:T(4,128)(2,1)S(1)} fusion(bf16[4096,512]{1,0:T(8,128)(2,1)} %param.13, bf16[4,4096]{1,0:T(4,128)(2,1)S(1)} %copy-done.5, f32[4096]{0:T(1024)S(1)} %copy-done.6, f32[4]{0:T(128)S(1)} %add_rsqrt_fusion.2), kind=kOutput, calls=%fused_computation.27 | convolution fusion | flops 16844800 | bytes 4247568 | tf_op jit(solution)/shard_map/dot_general | solution.py:54
  57.5 2.9 %fusion.19 = f32[4,512]{1,0:T(4,128)S(1)} fusion(bf16[4096,512]{1,0:T(8,128)(2,1)} %param.12, bf16[4,4096]{1,0:T(4,128)(2,1)S(1)} %copy-done.5, f32[4096]{0:T(1024)S(1)} %copy-done.6, f32[4]{0:T(128)S(1)} %add_rsqrt_fusion.2), kind=kOutput, calls=%fused_computation.26 | convolution fusion | flops 16846848 | bytes 4251664 | tf_op jit(solution)/shard_map/dot_general | solution.py:49
  62.5 17.2 %all-to-all-done.1 = f32[1,4,4,128,128]{4,2,1,0,3:T(4,128)S(1)} async-done(((f32[1,4,4,128,128]{4,2,1,0,3:T(4,128)}), f32[1,4,4,128,128]{4,2,1,0,3:T(4,128)S(1)}, u32[]{:S(2)}, u32[]{:S(2)}) %all-to-all-start.1) | async-done | bytes 1048608 | tf_op jit(solution)/shard_map/all_to_all | solution.py:42
  79.7 0.8 multiply_reduce_fusion.1
  80.8 0.7 copy.29
  81.8 10.0 %psum.7 = f32[4,4,128]{2,1,0:T(4,128)S(1)} all-reduce(f32[4,4,128]{2,1,0:T(4,128)S(1)} %bitcast.77), channel_id=1, replica_groups=mesh['gr'=2,'sp'=4,'tp'=4] {'sp'}, use_global_device_ids=true, to_apply=%region_7.8 | all-reduce | flops 2048 | bytes 16384 | tf_op jit(solution)/shard_map/psum | solution.py:63
  91.9 0.7 multiply_multiply_fusion
  (49 shorter events, 3.9 us)
Async XLA Ops:
  0.6 80.9 %copy-start = (bf16[4,4,32]{2,1,0:T(4,128)(2,1)S(1)}, bf16[4,4,32]{2,1,0:T(4,128)(2,1)}, u32[]{:S(2)}) copy-start(bf16[4,4,32]{2,1,0:T(4,128)(2,1)} %param.16) | copy-start | bytes 3076
  0.6 10.7 %copy-start.7 = (f32[4,128]{1,0:T(4,128)S(1)}, f32[4,128]{1,0:T(4,128)}, u32[]{:S(2)}) copy-start(f32[4,128]{1,0:T(4,128)} %param.14) | copy-start | bytes 6148
  0.7 10.7 %copy-start.8 = (f32[4,192,4]{1,2,0:T(4,128)S(1)}, f32[4,192,4]{1,2,0:T(4,128)}, u32[]{:S(2)}) copy-start(f32[4,192,4]{1,2,0:T(4,128)} %param.15) | copy-start | bytes 36868
  7.1 4.6 %copy-start.1 = (bf16[4,192,4096]{2,1,0:T(8,128)(2,1)S(1)}, bf16[4,192,4096]{2,1,0:T(8,128)(2,1)}, u32[]{:S(2)}) copy-start(bf16[4,192,4096]{2,1,0:T(8,128)(2,1)} %param.9) | copy-start | bytes 18874372
  7.1 4.6 %copy-start.6 = (f32[4096]{0:T(1024)S(1)}, f32[4096]{0:T(1024)}, u32[]{:S(2)}) copy-start(f32[4096]{0:T(1024)} %param.11) | copy-start | bytes 49156
  18.1 1.2 %copy-start.4 = (f32[4,192,4,128]{3,1,2,0:T(8,128)}, f32[4,192,4,128]{3,1,2,0:T(8,128)S(1)}, u32[]{:S(2)}) copy-start(f32[4,192,4,128]{3,1,2,0:T(8,128)S(1)} %get-tuple-element.9) | copy-start | bytes 4718596
  21.0 28.4 %all-to-all-start = ((f32[4,1,512]{2,1,0:T(1,128)}), f32[4,1,512]{2,1,0:T(1,128)S(1)}, u32[]{:S(2)}, u32[]{:S(2)}) async-start(f32[4,1,512]{2,1,0:T(1,128)} %reshape.91), calls=%async_computation | async-start | bytes 16384 | tf_op jit(solution)/shard_map/all_to_all | solution.py:43
  27.7 6.7 %slice-start = ((s8[6291456]{0:T(1024)(128)(4,1)}), s8[2097152]{0:T(1024)(128)(4,1)S(1)}, s32[]{:S(2)}) async-start(s8[6291456]{0:T(1024)(128)(4,1)} %bitcast.63), calls=%async_computation.2 | async-start | bytes 4194304
  29.3 1.4 %copy-start.2 = (f32[4,128,4,2,128]{1,3,2,4,0:T(2,128)}, f32[4,128,4,2,128]{1,3,2,4,0:T(2,128)S(1)}, u32[]{:S(2)}) copy-start(f32[4,128,4,2,128]{1,3,2,4,0:T(2,128)S(1)} %fusion.8) | copy-start | bytes 6291460
  30.7 3.6 %slice-start.1 = ((s8[6291456]{0:T(1024)(128)(4,1)}), s8[4194304]{0:T(1024)(128)(4,1)S(1)}, s32[]{:S(2)}) async-start(s8[6291456]{0:T(1024)(128)(4,1)} %bitcast.63), calls=%async_computation.3 | async-start | bytes 8388608
  37.1 8.4 %copy-start.3 = (f32[4,128,4,2,128]{1,4,3,2,0:T(8,128)S(1)}, f32[4,128,4,2,128]{1,4,3,2,0:T(8,128)}, u32[]{:S(2)}) copy-start(f32[4,128,4,2,128]{1,4,3,2,0:T(8,128)} %copy.24) | copy-start | bytes 6291460
  45.5 2.1 %copy-start.5 = (bf16[4,4096]{1,0:T(4,128)(2,1)S(1)}, bf16[4,4096]{1,0:T(4,128)(2,1)}, u32[]{:S(2)}) copy-start(bf16[4,4096]{1,0:T(4,128)(2,1)} %param.10) | copy-start | bytes 98308
  49.5 30.3 %all-to-all-start.1 = ((f32[1,4,4,128,128]{4,2,1,0,3:T(4,128)}), f32[1,4,4,128,128]{4,2,1,0,3:T(4,128)S(1)}, u32[]{:S(2)}, u32[]{:S(2)}) async-start(f32[1,4,4,128,128]{4,2,1,0,3:T(4,128)} %copy.26), calls=%async_computation.1 | async-start | bytes 2097152 | tf_op jit(solution)/shard_map/all_to_all | solution.py:42
  62.3 29.6 %copy-start.9 = (f32[4,128]{1,0:T(4,128)S(1)}, f32[4,128]{1,0:T(4,128)}, u32[]{:S(2)}) copy-start(f32[4,128]{1,0:T(4,128)} %param.17) | copy-start | bytes 6148
where the time goes:
time: 93.1 us; the launch traced here: 92.6 us
  matrix products  21.2 us (23%)
  local copies, waits for them, and re-layouts  17.7 us (19%)
  waiting for transfers between devices  17.2 us (18%)
  other arithmetic  14.2 us (15%)
  starting transfers between devices  11.4 us (12%)
  blocking collectives  9.98 us (11%)
    all_to_all x1, waiting for transfers between devices, local(): lax.all_to_all(pieces[None], 'sp', split_axis=3, concat_axis=0, tiled=True)  17.2 us
    psum x1, blocking collectives, local(): read_raw = lax.psum(partial_value, 'sp')  9.98 us
    dot_general x1, matrix products, local(): jnp.dot(unit_norm_rows, w_value, preferred_element_type=jnp.float32)  6.62 us
    dot_general x1, local copies, waits for them, and re-layouts, local(): jnp.dot(unit_norm_rows, w_forget, preferred_element_type=jnp.float32)  6.42 us
    dot_general x1, matrix products, local(): jnp.dot(unit_norm_rows, w_forget, preferred_element_type=jnp.float32)  6.41 us
    all_to_all x1, starting transfers between devices, local(): lax.all_to_all(totals[None], 'sp', split_axis=3, concat_axis=0, tiled=True)  6.35 us
    all_to_all x1, starting transfers between devices, local(): lax.all_to_all(pieces[None], 'sp', split_axis=3, concat_axis=0, tiled=True)  5.1 us
    unnamed x27, local copies, waits for them, and re-layouts  4.8 us
  transfers between devices with their start and end apart: 2, of which 1 were waited for; matrix products, arithmetic and copies ran while one was open for 31% of the time, Pallas kernels for 0%

commit v1 on v0

--- a/solution.py
+++ b/solution.py
@@ -60,7 +60,9 @@
     partial_value = jnp.einsum(
         "shi,shij->shj", query.astype(jnp.float32), updated, precision=lax.Precision.HIGHEST
     )
-    read_raw = lax.psum(partial_value, "sp")
+    read_raw = partial_value
+    for hop in (1, 2):
+        read_raw = read_raw + lax.ppermute(read_raw, "sp", [(dev, dev ^ hop) for dev in range(4)])
     read = (
         read_raw
         * lax.rsqrt(jnp.mean(read_raw * read_raw, axis=-1, keepdims=True) + epsilon)

time: 93.1 us -> 90.7 us (0.974)
  blocking collectives: 9.98 us -> 0 us
  waiting for transfers between devices: 17.2 us -> 24.7 us
    psum x1 -> x0, blocking collectives: 9.98 us -> none  [local(): read_raw = lax.psum(partial_value, 'sp')]
    ppermute x0 -> x2, waiting for transfers between devices: none -> 7.49 us  [local(): lax.ppermute(read_raw, 'sp', [(dev, dev ^ hop) for dev in range(4)])]
  transfers between devices with their start and end apart: 2 -> 4, of which waited for: 1 -> 3; matrix products, arithmetic and copies ran while one was open for 31% -> 32% of each run, Pallas kernels for 0% -> 0%
where the time goes in v1:
time: 90.7 us; the launch traced here: 90.2 us
  waiting for transfers between devices  24.7 us (27%)
  matrix products  21.2 us (23%)
  local copies, waits for them, and re-layouts  17.7 us (20%)
  other arithmetic  14.2 us (16%)
  starting transfers between devices  11.5 us (13%)
    all_to_all x1, waiting for transfers between devices, local(): lax.all_to_all(pieces[None], 'sp', split_axis=3, concat_axis=0, tiled=True)  17.2 us
    ppermute x2, waiting for transfers between devices, local(): lax.ppermute(read_raw, 'sp', [(dev, dev ^ hop) for dev in range(4)])  7.49 us
    dot_general x1, matrix products, local(): jnp.dot(unit_norm_rows, w_value, preferred_element_type=jnp.float32)  6.62 us
    dot_general x1, local copies, waits for them, and re-layouts, local(): jnp.dot(unit_norm_rows, w_forget, preferred_element_type=jnp.float32)  6.42 us
    dot_general x1, matrix products, local(): jnp.dot(unit_norm_rows, w_forget, preferred_element_type=jnp.float32)  6.41 us
    all_to_all x1, starting transfers between devices, local(): lax.all_to_all(totals[None], 'sp', split_axis=3, concat_axis=0, tiled=True)  6.35 us
    all_to_all x1, starting transfers between devices, local(): lax.all_to_all(pieces[None], 'sp', split_axis=3, concat_axis=0, tiled=True)  5.1 us
    unnamed x27, local copies, waits for them, and re-layouts  4.8 us
  transfers between devices with their start and end apart: 4, of which 3 were waited for; matrix products, arithmetic and copies ran while one was open for 32% of the time, Pallas kernels for 0%

profile of v1, /device:TPU:0, one launch (start us, length us, event | category | flops | bytes accessed | tf_op | source)
XLA Modules:
  0.0 90.2 jit_solution(6845965586532249835)
XLA Ops:
  0.7 6.4 %copy.34 = bf16[512,4096]{1,0:T(8,128)(2,1)} copy(bf16[512,4096]{0,1:T(8,128)(2,1)} %bitcast.65) | data formatting | bytes 8388608 | tf_op jit(solution)/shard_map/dot_general | solution.py:27
  7.1 4.2 %multiply_reduce_fusion = f32[4,192]{1,0:T(4,128)S(1)} fusion(bf16[4,192,4096]{2,1,0:T(8,128)(2,1)} %param.9), kind=kLoop, calls=%fused_computation.4 | loop fusion | flops 9436416 | bytes 6294528 | tf_op jit(solution)/shard_map/reduce_sum | solution.py:11
  11.7 6.4 %fusion.15 = (f32[4,128,4,192]{1,3,2,0:T(8,128)S(1)}, f32[4,192,4,128]{3,1,2,0:T(8,128)S(1)}) fusion(f32[4,4,192]{2,1,0:T(4,128)S(1)} %bitcast.80, f32[128,4]{0,1:T(4,128)S(1)} %bitcast.79, bf16[4,128,4096,1]{2,1,0,3:T(8,128)(2,1)} %bitcast.70, f32[4096]{0:T(1024)S(1)} %copy-done.6, f32[4,192]{1,0:T(4,128)S(1)} %add_rsqrt_fusion, ...), kind=kOutput, calls=%fused_computation.19 | convolution fusion | flops 3235774464 | bytes 13665280 | tf_op jit(solution)/shard_map/dot_general | solution.py:27
  18.1 1.1 %copy-done.4 = f32[4,192,4,128]{3,1,2,0:T(8,128)} copy-done((f32[4,192,4,128]{3,1,2,0:T(8,128)}, f32[4,192,4,128]{3,1,2,0:T(8,128)S(1)}, u32[]{:S(2)}) %copy-start.4) | copy-done | bytes 1572888
  19.3 0.7 add_reduce_fusion
  20.2 0.9 reshape.91
  21.0 6.3 %all-to-all-start = ((f32[4,1,512]{2,1,0:T(1,128)}), f32[4,1,512]{2,1,0:T(1,128)S(1)}, u32[]{:S(2)}, u32[]{:S(2)}) async-start(f32[4,1,512]{2,1,0:T(1,128)} %reshape.91), calls=%async_computation | async-start | bytes 16384 | tf_op jit(solution)/shard_map/all_to_all | solution.py:43
  27.7 1.6 %fusion.8 = f32[4,128,4,2,128]{1,3,2,4,0:T(2,128)S(1)} fusion(f32[4,128,4,2,128]{1,4,3,2,0:T(8,128)S(1)} %bitcast.68), kind=kOutput, calls=%fused_computation.10 | output fusion | flops 66584576 | bytes 4194304 | tf_op jit(solution)/shard_map/reduce-window
  29.3 1.3 %copy-done.2 = f32[4,128,4,2,128]{1,3,2,4,0:T(2,128)} copy-done((f32[4,128,4,2,128]{1,3,2,4,0:T(2,128)}, f32[4,128,4,2,128]{1,3,2,4,0:T(2,128)S(1)}, u32[]{:S(2)}) %copy-start.2) | copy-done | bytes 2097176
  30.8 1.9 %broadcast_add_fusion = f32[4,128,1,8,128]{1,3,2,4,0:T(8,128)S(1)} fusion(f32[4,128,1,8,128]{1,3,2,4,0:T(8,128)} %bitcast.66, f32[4,128,1,8]{1,3,2,0:T(8,128)S(1)} %bitcast.76), kind=kLoop, calls=%fused_computation.29 | loop fusion | flops 524288 | bytes 4210688 | tf_op jit(solution)/shard_map/reduce_window_sum
  32.6 1.7 %copy.24 = f32[4,128,4,2,128]{1,4,3,2,0:T(8,128)} copy(f32[4,128,4,2,128]{1,3,2,4,0:T(2,128)S(1)} %bitcast.67) | data formatting | bytes 4194304 | tf_op jit(solution)/shard_map/reduce_window_sum
  34.4 2.7 %fusion.1 = bf16[768,4096]{1,0:T(8,128)(2,1)S(1)} fusion(f32[4096]{0:T(1024)S(1)} %copy-done.6, f32[768]{0:T(1024)S(1)} %rsqrt.29, bf16[4,192,4096]{2,1,0:T(8,128)(2,1)S(1)} %bitcast.64), kind=kLoop, calls=%fused_computation.2 | loop fusion | flops 12582912 | bytes 12602368 | tf_op jit(solution)/shard_map/convert_element_type | solution.py:12
  37.1 6.6 %convolution_convert_fusion = bf16[768,512]{1,0:T(8,128)(2,1)} fusion(bf16[768,4096]{1,0:T(8,128)(2,1)S(1)} %fusion.1, bf16[4096,512]{1,0:T(8,128)(2,1)} %param.13), kind=kOutput, calls=%fused_computation.22 | convolution fusion | flops 3221618688 | bytes 11272192 | tf_op jit(solution)/shard_map/dot_general | solution.py:30
  43.8 1.7 %reshape.84 = bf16[4,192,4,128]{3,2,1,0:T(4,128)(2,1)S(1)} reshape(bf16[768,512]{1,0:T(8,128)(2,1)} %convolution_convert_fusion) | data formatting | bytes 1572864 | tf_op jit(solution)/shard_map/reshape | solution.py:33
  45.5 2.1 %convolution_bitcast_fusion = f32[1,4,4,128,128]{4,3,2,1,0:T(8,128)S(1)} fusion(f32[4,256,4,128]{3,1,2,0:T(8,128)S(1)} %bitcast.69, f32[4,192,4,128]{3,1,2,0:T(8,128)} %copy-done.4, bf16[4,192,4,128]{3,2,1,0:T(4,128)(2,1)S(1)} %reshape.84, f32[4,4,128]{2,1,0:T(4,128)S(1)} %add_reduce_fusion, f32[4,128]{1,0:T(4,128)S(1)} %copy-done.7), kind=kOutput, calls=%fused_computation.23 | convolution fusion | flops 102236160 | bytes 4990976 | tf_op jit(solution)/shard_map/sthi,sthj->shij/dot_general | solution.py:39
  47.8 1.7 %copy.26 = f32[1,4,4,128,128]{4,2,1,0,3:T(4,128)} copy(f32[1,4,4,128,128]{4,3,2,1,0:T(8,128)S(1)} %convolution_bitcast_fusion) | data formatting | bytes 2097152 | tf_op jit(solution)/shard_map/broadcast_in_dim | solution.py:42
  49.5 5.1 %all-to-all-start.1 = ((f32[1,4,4,128,128]{4,2,1,0,3:T(4,128)}), f32[1,4,4,128,128]{4,2,1,0,3:T(4,128)S(1)}, u32[]{:S(2)}, u32[]{:S(2)}) async-start(f32[1,4,4,128,128]{4,2,1,0,3:T(4,128)} %copy.26), calls=%async_computation.1 | async-start | bytes 2097152 | tf_op jit(solution)/shard_map/all_to_all | solution.py:42
  54.6 2.9 %convolution_convert_fusion.1 = bf16[4,512]{1,0:T(4,128)(2,1)S(1)} fusion(bf16[4096,512]{1,0:T(8,128)(2,1)} %param.13, bf16[4,4096]{1,0:T(4,128)(2,1)S(1)} %copy-done.5, f32[4096]{0:T(1024)S(1)} %copy-done.6, f32[4]{0:T(128)S(1)} %add_rsqrt_fusion.2), kind=kOutput, calls=%fused_computation.27 | convolution fusion | flops 16844800 | bytes 4247568 | tf_op jit(solution)/shard_map/dot_general | solution.py:54
  57.5 2.9 %fusion.19 = f32[4,512]{1,0:T(4,128)S(1)} fusion(bf16[4096,512]{1,0:T(8,128)(2,1)} %param.12, bf16[4,4096]{1,0:T(4,128)(2,1)S(1)} %copy-done.5, f32[4096]{0:T(1024)S(1)} %copy-done.6, f32[4]{0:T(128)S(1)} %add_rsqrt_fusion.2), kind=kOutput, calls=%fused_computation.26 | convolution fusion | flops 16846848 | bytes 4251664 | tf_op jit(solution)/shard_map/dot_general | solution.py:49
  62.5 17.2 %all-to-all-done.1 = f32[1,4,4,128,128]{4,2,1,0,3:T(4,128)S(1)} async-done(((f32[1,4,4,128,128]{4,2,1,0,3:T(4,128)}), f32[1,4,4,128,128]{4,2,1,0,3:T(4,128)S(1)}, u32[]{:S(2)}, u32[]{:S(2)}) %all-to-all-start.1) | async-done | bytes 1048608 | tf_op jit(solution)/shard_map/all_to_all | solution.py:42
  79.7 0.8 multiply_reduce_fusion.1
  81.2 3.6 %collective-permute-done = f32[4,4,128]{2,1,0:T(4,128)S(1)} collective-permute-done((f32[4,4,128]{2,1,0:T(4,128)S(1)}, f32[4,4,128]{2,1,0:T(4,128)S(1)}, u32[]{:S(2)}, u32[]{:S(2)}) %collective-permute-start) | collective-permute-done | bytes 8224 | tf_op jit(solution)/shard_map/ppermute | solution.py:65
  84.9 0.7 copy.29
  85.6 3.9 %collective-permute-done.1 = f32[4,4,128]{2,1,0:T(4,128)S(1)} collective-permute-done((f32[4,4,128]{2,1,0:T(4,128)S(1)}, f32[4,4,128]{2,1,0:T(4,128)S(1)}, u32[]{:S(2)}, u32[]{:S(2)}) %collective-permute-start.1) | collective-permute-done | bytes 8224 | tf_op jit(solution)/shard_map/ppermute | solution.py:65
  (53 shorter events, 4.7 us)
Async XLA Ops:
  0.6 80.2 %copy-start = (bf16[4,4,32]{2,1,0:T(4,128)(2,1)S(1)}, bf16[4,4,32]{2,1,0:T(4,128)(2,1)}, u32[]{:S(2)}) copy-start(bf16[4,4,32]{2,1,0:T(4,128)(2,1)} %param.16) | copy-start | bytes 3076
  0.6 10.7 %copy-start.7 = (f32[4,128]{1,0:T(4,128)S(1)}, f32[4,128]{1,0:T(4,128)}, u32[]{:S(2)}) copy-start(f32[4,128]{1,0:T(4,128)} %param.14) | copy-start | bytes 6148
  0.7 10.7 %copy-start.8 = (f32[4,192,4]{1,2,0:T(4,128)S(1)}, f32[4,192,4]{1,2,0:T(4,128)}, u32[]{:S(2)}) copy-start(f32[4,192,4]{1,2,0:T(4,128)} %param.15) | copy-start | bytes 36868
  7.1 4.6 %copy-start.1 = (bf16[4,192,4096]{2,1,0:T(8,128)(2,1)S(1)}, bf16[4,192,4096]{2,1,0:T(8,128)(2,1)}, u32[]{:S(2)}) copy-start(bf16[4,192,4096]{2,1,0:T(8,128)(2,1)} %param.9) | copy-start | bytes 18874372
  7.1 4.6 %copy-start.6 = (f32[4096]{0:T(1024)S(1)}, f32[4096]{0:T(1024)}, u32[]{:S(2)}) copy-start(f32[4096]{0:T(1024)} %param.11) | copy-start | bytes 49156
  18.1 1.2 %copy-start.4 = (f32[4,192,4,128]{3,1,2,0:T(8,128)}, f32[4,192,4,128]{3,1,2,0:T(8,128)S(1)}, u32[]{:S(2)}) copy-start(f32[4,192,4,128]{3,1,2,0:T(8,128)S(1)} %get-tuple-element.11) | copy-start | bytes 4718596
  21.0 28.4 %all-to-all-start = ((f32[4,1,512]{2,1,0:T(1,128)}), f32[4,1,512]{2,1,0:T(1,128)S(1)}, u32[]{:S(2)}, u32[]{:S(2)}) async-start(f32[4,1,512]{2,1,0:T(1,128)} %reshape.91), calls=%async_computation | async-start | bytes 16384 | tf_op jit(solution)/shard_map/all_to_all | solution.py:43
  27.7 6.7 %slice-start = ((s8[6291456]{0:T(1024)(128)(4,1)}), s8[2097152]{0:T(1024)(128)(4,1)S(1)}, s32[]{:S(2)}) async-start(s8[6291456]{0:T(1024)(128)(4,1)} %bitcast.63), calls=%async_computation.2 | async-start | bytes 4194304
  29.3 1.4 %copy-start.2 = (f32[4,128,4,2,128]{1,3,2,4,0:T(2,128)}, f32[4,128,4,2,128]{1,3,2,4,0:T(2,128)S(1)}, u32[]{:S(2)}) copy-start(f32[4,128,4,2,128]{1,3,2,4,0:T(2,128)S(1)} %fusion.8) | copy-start | bytes 6291460
  30.7 3.6 %slice-start.1 = ((s8[6291456]{0:T(1024)(128)(4,1)}), s8[4194304]{0:T(1024)(128)(4,1)S(1)}, s32[]{:S(2)}) async-start(s8[6291456]{0:T(1024)(128)(4,1)} %bitcast.63), calls=%async_computation.3 | async-start | bytes 8388608
  37.1 8.4 %copy-start.3 = (f32[4,128,4,2,128]{1,4,3,2,0:T(8,128)S(1)}, f32[4,128,4,2,128]{1,4,3,2,0:T(8,128)}, u32[]{:S(2)}) copy-start(f32[4,128,4,2,128]{1,4,3,2,0:T(8,128)} %copy.24) | copy-start | bytes 6291460
  45.5 2.1 %copy-start.5 = (bf16[4,4096]{1,0:T(4,128)(2,1)S(1)}, bf16[4,4096]{1,0:T(4,128)(2,1)}, u32[]{:S(2)}) copy-start(bf16[4,4096]{1,0:T(4,128)(2,1)} %param.10) | copy-start | bytes 98308
  49.5 30.3 %all-to-all-start.1 = ((f32[1,4,4,128,128]{4,2,1,0,3:T(4,128)}), f32[1,4,4,128,128]{4,2,1,0,3:T(4,128)S(1)}, u32[]{:S(2)}, u32[]{:S(2)}) async-start(f32[1,4,4,128,128]{4,2,1,0,3:T(4,128)} %copy.26), calls=%async_computation.1 | async-start | bytes 2097152 | tf_op jit(solution)/shard_map/all_to_all | solution.py:42
  62.3 27.2 %copy-start.9 = (f32[4,128]{1,0:T(4,128)S(1)}, f32[4,128]{1,0:T(4,128)}, u32[]{:S(2)}) copy-start(f32[4,128]{1,0:T(4,128)} %param.17) | copy-start | bytes 6148
  81.2 3.7 %collective-permute-start = (f32[4,4,128]{2,1,0:T(4,128)S(1)}, f32[4,4,128]{2,1,0:T(4,128)S(1)}, u32[]{:S(2)}, u32[]{:S(2)}) collective-permute-start(f32[4,4,128]{2,1,0:T(4,128)S(1)} %bitcast.77), channel_id=1, source_target_pairs={{0,4},{4,0},{8,12},{12,8},{1,5},{5,1},{9,13},{13,9},{2,6},{6,2},{1... | collective-permute-start | bytes 24584 | tf_op jit(solution)/shard_map/ppermute | solution.py:65
  84.9 4.5 %collective-permute-start.1 = (f32[4,4,128]{2,1,0:T(4,128)S(1)}, f32[4,4,128]{2,1,0:T(4,128)S(1)}, u32[]{:S(2)}, u32[]{:S(2)}) collective-permute-start(f32[4,4,128]{2,1,0:T(4,128)S(1)} %add.79), channel_id=1, source_target_pairs={{0,8},{4,12},{8,0},{12,4},{1,9},{5,13},{9,1},{13,5},{2,10},{6,14},... | collective-permute-start | bytes 24584 | tf_op jit(solution)/shard_map/ppermute | solution.py:65
